TPU v7x, 32 devices: a whole 2x2x4 slice. The times are simulated.
32 devices in a mesh: sp: 16 (over z, y, x), tp: 2 (over core).
Axes of the slice: x: 2, y: 2, z: 4, core: 2. Of those that a mesh axis runs over, the one named last changes fastest.
Arguments:
- tokens: bfloat16 [8192, 2048], P('sp', 'tp'), may hold values from -6 to 6
- input_gain: bfloat16 [2048], P('tp'), may hold values from 0.099609375 to 1.8984375
- query_weight: bfloat16 [2048, 1024], P(None, 'tp'), may hold values from -10 to 10
- key_weight: bfloat16 [2048, 1024], P(None, 'tp'), may hold values from -10 to 10
- value_weight: bfloat16 [2048, 1024], P(None, 'tp'), may hold values from -0.125 to 0.125
- pool_in_weight: bfloat16 [2048, 1024], P(None, 'tp'), may hold values from -0.125 to 0.125
- log_gates: float32 [8, 8192], P('tp'), may hold values from -8192 to 0, as said below
- pool_weight: bfloat16 [8, 128, 128], P('tp'), may hold values from -0.5 to 0.5
- pool_scale: float32 [1024], P('tp'), may hold values from 0.1 to 1.9
- attention_out: bfloat16 [1024, 2048], P('tp'), may hold values from -16 to 16
- pooling_out: bfloat16 [1024, 2048], P('tp'), may hold values from -16 to 16
- final_gain: float32 [2048], P('tp'), may hold values from 0.1 to 1.9
Outputs:
- layer_out: bfloat16 [8192, 2048], P('sp', 'tp')
Inputs may be any that keep to these rules, and one draw needn't show every extreme that they name: `log_gates`: each row does not increase along positions.
All inputs are finite; a program needn't handle non-finite values.
Results may differ from a plain program's by a relative error of at most 0.015.
Values may be sent and summed in bfloat16 or wider, within the bound.
A program may use at most 128 MiB of HBM per device.

v0:
```python
import jax
import jax.numpy as jnp
from jax import lax
from jax.sharding import PartitionSpec as P

WINDOW_MAX = 16
very_low = -1e30
epsilon = 1e-06
key_span = 2048


def passed_along(block, axis, distance):
    devices = range(lax.axis_size(axis))
    route = [(i - distance, i) for i in devices if i - distance in devices]
    return lax.ppermute(block, axis, route)


def attend_block(state, queries, query_gate, query_first, keys, values, key_gate, key_first):
    maxima, totals, summed = state
    head_size = queries.shape[2]
    scores = jnp.einsum(
        "thd,shd->ths", queries, keys, preferred_element_type=jnp.float32
    ) * head_size ** (-0.5)
    scores = scores + query_gate[:, :, None] - key_gate[None, :, :]
    query_rows = query_first + jnp.arange(queries.shape[0], dtype=jnp.int32)
    key_rows = key_first + jnp.arange(keys.shape[0], dtype=jnp.int32)
    allowed = (query_rows[:, None] >= key_rows[None, :])[:, None, :]
    scores = jnp.where(allowed, scores, very_low)
    new_max = jnp.maximum(maxima, jnp.max(scores, axis=2))
    weights = jnp.where(allowed, jnp.exp(scores - new_max[:, :, None]), 0.0)
    factor = jnp.exp(maxima - new_max)
    totals = factor * totals + jnp.sum(weights, axis=2)
    summed = factor[:, :, None] * summed + jnp.einsum(
        "ths,shd->thd", weights.astype(jnp.bfloat16), values, preferred_element_type=jnp.float32
    )
    return (new_max, totals, summed)


def attend(state, queries, query_gate, query_first, keys, values, log_gates):
    count = keys.shape[0]
    heads = queries.shape[1]
    head_size = queries.shape[2]
    span = count
    for halving in range(24):
        if span > key_span and span % 2 == 0:
            span = span // 2
    pieces = count // span
    keys_blocked = keys.reshape(pieces, span, heads, head_size)
    values_blocked = values.reshape(pieces, span, heads, head_size)
    gates_blocked = log_gates.reshape(heads, pieces, span).transpose(1, 0, 2)
    block_starts = span * jnp.arange(pieces, dtype=jnp.int32)

    def step(carry, block):
        return (
            attend_block(
                carry, queries, query_gate, query_first, block[0], block[1], block[2], block[3]
            ),
            None,
        )

    state, unused = lax.scan(
        step, state, (keys_blocked, values_blocked, gates_blocked, block_starts)
    )
    return state


def body(
    tokens,
    input_gain,
    query_weight,
    key_weight,
    value_weight,
    pool_in_weight,
    log_gates,
    pool_weight,
    pool_scale,
    attention_out,
    pooling_out,
    final_gain,
):
    tok_rows = tokens.shape[0]
    width = query_weight.shape[0]
    groups = pool_weight.shape[0]
    head_size = pool_weight.shape[1]
    heads = log_gates.shape[0]
    attention_width = query_weight.shape[1]
    pool_width = pool_in_weight.shape[1]
    sequence_index = lax.axis_index("sp")
    first_row = sequence_index * tok_rows
    last_row = first_row + tok_rows - 1
    part = lax.all_gather(tokens, "tp", axis=1, tiled=True)
    gain_part = lax.all_gather(input_gain.reshape(1, -1), "tp", axis=1, tiled=True)
    widened = part.astype(jnp.float32)
    scaled = (widened * gain_part.astype(jnp.float32)).astype(jnp.bfloat16)

    def product(weight):
        return jnp.dot(scaled, weight, preferred_element_type=jnp.float32)

    inverse = lax.rsqrt(jnp.sum(widened * widened, axis=1) / width + epsilon)[:, None]
    query = (
        (product(query_weight) * inverse).astype(jnp.bfloat16).reshape(tok_rows, heads, head_size)
    )
    keys = (product(key_weight) * inverse).astype(jnp.bfloat16)
    values = (product(value_weight) * inverse).astype(jnp.bfloat16)
    pool_input = (product(pool_in_weight) * inverse).astype(jnp.bfloat16)
    query_gate = lax.dynamic_slice_in_dim(log_gates, first_row, tok_rows, 1).T
    state = (
        jnp.full((tok_rows, heads), very_low, jnp.float32),
        jnp.zeros((tok_rows, heads), jnp.float32),
        jnp.zeros((tok_rows, heads, head_size), jnp.float32),
    )
    carry = state
    pieces = (
        lax.all_gather(keys, "sp", axis=0, tiled=True),
        lax.all_gather(values, "sp", axis=0, tiled=True),
    )
    state = lax.cond(
        jnp.int32(0) > last_row,
        lambda: carry,
        lambda: attend(carry, query, query_gate, first_row, pieces[0], pieces[1], log_gates),
    )
    maxima, totals, summed = state
    attended = (summed / totals[:, :, None]).astype(jnp.bfloat16).reshape(tok_rows, attention_width)
    rim = passed_along(pool_input[tok_rows - (WINDOW_MAX - 1) :], "sp", 1)
    extended = jnp.concatenate([rim, pool_input], axis=0).astype(jnp.float32)
    column = jnp.arange(pool_width, dtype=jnp.int32)
    group_number = lax.axis_index("tp") * groups + column // head_size
    window = jnp.left_shift(jnp.full((pool_width,), 2, jnp.int32), group_number % 4)
    sums = extended
    span = 1
    chosen = jnp.zeros((tok_rows, pool_width), jnp.float32)
    for level in range(4):
        sums = sums[span:] + sums[:-span]
        span = span * 2
        offset_rows = WINDOW_MAX - span
        chosen = jnp.where(
            window[None, :] == span, sums[offset_rows : offset_rows + tok_rows], chosen
        )
    element_locations = first_row + jnp.arange(tok_rows, dtype=jnp.int32)
    counts = jnp.minimum(window[None, :], element_locations[:, None] + 1).astype(jnp.float32)
    departure = (chosen / counts - pool_input.astype(jnp.float32)).astype(jnp.bfloat16)
    mapped = jnp.einsum(
        "tgc,gcd->tgd",
        departure.reshape(tok_rows, groups, head_size),
        pool_weight,
        preferred_element_type=jnp.float32,
    )
    pooled = (mapped.reshape(tok_rows, pool_width) * pool_scale).astype(jnp.bfloat16)
    numbers = (((0,), (1,)), ((), ()))
    mixed = lax.psum_scatter(
        (
            lax.dot_general(attention_out, attended, numbers, preferred_element_type=jnp.float32)
            + lax.dot_general(pooling_out, pooled, numbers, preferred_element_type=jnp.float32)
        ).astype(jnp.bfloat16),
        "tp",
        scatter_dimension=0,
        tiled=True,
    ).astype(jnp.float32)
    squares = lax.psum(jnp.sum(mixed * mixed, axis=0), "tp")
    out_inverse = lax.rsqrt(squares / width + epsilon)
    return (mixed * out_inverse[None, :] * final_gain[:, None]).T.astype(jnp.bfloat16)


def solution(mesh):
    return jax.shard_map(
        body,
        mesh=mesh,
        in_specs=(
            P("sp", "tp"),
            P("tp"),
            P(None, "tp"),
            P(None, "tp"),
            P(None, "tp"),
            P(None, "tp"),
            P("tp", None),
            P("tp", None, None),
            P("tp"),
            P("tp", None),
            P("tp", None),
            P("tp"),
        ),
        out_specs=P("sp", "tp"),
        check_vma=False,
    )
```

profile of v0, /device:TPU:0, one launch (start us, length us, event | category | flops | bytes accessed | tf_op | source)
XLA Modules:
  0.0 463.4 jit_solution(7323547695319961552)
XLA Ops:
  6.5 0.7 all-gather.5.cloned.1.call-update
  7.3 2.1 all-gather
  9.4 12.8 %all-gather.5.cloned.1.call-done = bf16[512,2048]{1,0:T(8,128)(2,1)} async-done(((bf16[512,1024]{1,0:T(8,128)(2,1)}), bf16[512,2048]{1,0:T(8,128)(2,1)}) %all-gather.5.cloned.1.call-update) | async-done | bytes 2097168 | tf_op jit(solution)/shard_map/all_gather | solution.py:91
  22.2 2.2 fusion.25
  24.5 3.7 fusion.34
  28.2 4.3 fusion.37
  32.6 1.3 dynamic-slice_bitcast_fusion.1
  33.9 3.6 fusion.43
  37.6 3.6 collective-permute-start
  41.2 1.3 fusion.40
  43.4 0.7 copy-done.10
  44.1 0.8 fusion.54
  45.0 0.9 fusion.52
  45.9 95.9 %all-gather.7.cloned.1.call-done = bf16[8192,512]{1,0:T(8,128)(2,1)} async-done(((bf16[512,512]{1,0:T(8,128)(2,1)}), bf16[8192,512]{1,0:T(8,128)(2,1)}) %all-gather.7.cloned.1.call-update) | async-done | bytes 8388624 | tf_op jit(solution)/shard_map/all_gather | solution.py:114
  141.8 113.3 %all-gather.9.cloned.1.call-done = bf16[8192,512]{1,0:T(8,128)(2,1)} async-done(((bf16[512,512]{1,0:T(8,128)(2,1)}), bf16[8192,512]{1,0:T(8,128)(2,1)}) %all-gather.9.cloned.1.call-update) | async-done | bytes 8388624 | tf_op jit(solution)/shard_map/all_gather | solution.py:115
  255.0 181.5 %conditional.1 = (f32[512,4]{0,1:T(4,128)S(1)}, f32[512,4,128]{0,2,1:T(8,128)}) conditional(s32[]{:T(128)} %convert_element_type.58, (bf16[8192,512]{1,0:T(8,128)(2,1)}, bf16[8192,512]{1,0:T(8,128)(2,1)}, f32[4,8192]{1,0:T(4,128)}, bf16[512,512]{1,0:T(8,128)(2,1)S(1)}, s32[]{:T(128)}, /*index=5*/f32[512,4]{0,1:T(4,128)}) %tuple.17, () %tuple.18), branch_computations={%region_1.6_spmd, %region_6.7_spmd} | conditional | flops 2229023232 | bytes 112046448 | solution.py:117
  255.0 12.6 %reshape.108 = bf16[4,2048,4,128]{3,2,1,0:T(4,128)(2,1)} reshape(bf16[8192,512]{1,0:T(8,128)(2,1)} %get-tuple-element.75) | data formatting | bytes 16777216 | tf_op jit(solution)/shard_map/cond/branch_0_fun/reshape | solution.py:48
  267.6 12.5 %reshape.111 = bf16[4,2048,4,128]{3,2,1,0:T(4,128)(2,1)} reshape(bf16[8192,512]{1,0:T(8,128)(2,1)} %get-tuple-element.79) | data formatting | bytes 16777216 | tf_op jit(solution)/shard_map/cond/branch_0_fun/reshape | solution.py:49
  280.3 1.0 copy.25
  281.4 155.2 %while.14 = (s32[]{:T(128)}, f32[512,4]{0,1:T(4,128)S(1)}, f32[512,4]{0,1:T(4,128)S(1)}, f32[512,4,128]{0,2,1:T(8,128)}, s32[]{:T(128)}, /*index=5*/s32[4]{0:T(1...) while((s32[]{:T(128)}, f32[512,4]{0,1:T(4,128)S(1)}, ...), condition=%wide.region_5.5_spmd.clone, body=%wide.region_2.4_spmd.clone.sunk | while | flops 2229023232 | bytes 76361920 | solution.py:61
  281.4 0.7 dynamic_slice.32
  282.1 0.7 iota_add_fusion.5
  282.8 0.8 broadcast_compare_fusion.6
  283.6 4.1 constant_dynamic-slice_fusion.3
  287.6 0.8 dynamic-slice_bitcast_fusion.3
  288.4 7.7 %fusion.87 = (f32[512,4]{0,1:T(4,128)S(1)}, f32[4,2048,512]{2,1,0:T(8,128)}) fusion(f32[4,2048]{1,0:T(4,128)S(1)} %dynamic-slice_bitcast_fusion.3, f32[512,4]{0,1:T(4,128)S(1)} %get-tuple-element.303, pred[512,2048]{0,1:T(8,128)(4,1)S(1)} %broadcast_compare_fusion.6, bf16[512,4,128]{2,0,1:T(8,128)(2,1)S(1)} %copy-done.5, ...), kind=kOutput, calls=%fused_computation.6.clone.1 | convolution fusion | flops 1094711296 | bytes 20496384 | tf_op jit(solution)/shard_map/cond/branch_0_fun/while/body/eval_jaxpr/thd,shd->ths/dot_general | solution.py:21
  296.1 8.8 %fusion.88 = f32[512,4]{0,1:T(4,128)S(1)} fusion(f32[4,2048,512]{2,1,0:T(8,128)} %get-tuple-element.265, f32[512,4]{0,1:T(4,128)S(1)} %select_maximum_fusion.2, f32[4,2048]{1,0:T(4,128)S(1)} %dynamic-slice_bitcast_fusion.3, f32[512,4]{0,1:T(4,128)S(1)} %get-tuple-element.303, pred[512,2048]{0,1:T(8,128)(4,1)S(1)} %broadcast_compare_fusion.6), kind=kLoop, calls=%fused_computation.5.clone.1 | loop fusion | flops 29358080 | bytes 17883136 | tf_op jit(solution)/shard_map/cond/branch_0_fun/while/body/eval_jaxpr/reduce_sum | solution.py:32
  304.9 4.4 copy.46
  309.3 10.8 %fusion.90 = f32[512,4,128]{0,2,1:T(8,128)} fusion(f32[4,2048,512]{2,1,0:T(8,128)} %get-tuple-element.265, f32[512,4]{0,1:T(4,128)S(1)} %select_maximum_fusion.2, f32[4,2048]{1,0:T(4,128)S(1)} %dynamic-slice_bitcast_fusion.3, f32[512,4]{0,1:T(4,128)S(1)} %get-tuple-element.303, pred[512,2048]{0,1:T(8,128)(4,1)S(1)} %broadcast_compare_fusion.6, ...), kind=kOutput, calls=%fused_computation.14.clone.1 | convolution fusion | flops 1103888384 | bytes 22077440 | tf_op jit(solution)/shard_map/cond/branch_0_fun/while/body/eval_jaxpr/ths,shd->thd/dot_general | solution.py:33
  320.1 0.7 dynamic_slice.32
  320.7 0.7 iota_add_fusion.5
  321.4 0.8 broadcast_compare_fusion.6
  322.2 4.1 constant_dynamic-slice_fusion.3
  326.3 0.8 dynamic-slice_bitcast_fusion.3
  327.0 7.7 %fusion.87 = (f32[512,4]{0,1:T(4,128)S(1)}, f32[4,2048,512]{2,1,0:T(8,128)}) fusion(f32[4,2048]{1,0:T(4,128)S(1)} %dynamic-slice_bitcast_fusion.3, f32[512,4]{0,1:T(4,128)S(1)} %get-tuple-element.303, pred[512,2048]{0,1:T(8,128)(4,1)S(1)} %broadcast_compare_fusion.6, bf16[512,4,128]{2,0,1:T(8,128)(2,1)S(1)} %copy-done.5, ...), kind=kOutput, calls=%fused_computation.6.clone.1 | convolution fusion | flops 1094711296 | bytes 20496384 | tf_op jit(solution)/shard_map/cond/branch_0_fun/while/body/eval_jaxpr/thd,shd->ths/dot_general | solution.py:21
  334.7 8.8 %fusion.88 = f32[512,4]{0,1:T(4,128)S(1)} fusion(f32[4,2048,512]{2,1,0:T(8,128)} %get-tuple-element.265, f32[512,4]{0,1:T(4,128)S(1)} %select_maximum_fusion.2, f32[4,2048]{1,0:T(4,128)S(1)} %dynamic-slice_bitcast_fusion.3, f32[512,4]{0,1:T(4,128)S(1)} %get-tuple-element.303, pred[512,2048]{0,1:T(8,128)(4,1)S(1)} %broadcast_compare_fusion.6), kind=kLoop, calls=%fused_computation.5.clone.1 | loop fusion | flops 29358080 | bytes 17883136 | tf_op jit(solution)/shard_map/cond/branch_0_fun/while/body/eval_jaxpr/reduce_sum | solution.py:32
  343.5 4.4 copy.46
  347.9 11.0 %fusion.90 = f32[512,4,128]{0,2,1:T(8,128)} fusion(f32[4,2048,512]{2,1,0:T(8,128)} %get-tuple-element.265, f32[512,4]{0,1:T(4,128)S(1)} %select_maximum_fusion.2, f32[4,2048]{1,0:T(4,128)S(1)} %dynamic-slice_bitcast_fusion.3, f32[512,4]{0,1:T(4,128)S(1)} %get-tuple-element.303, pred[512,2048]{0,1:T(8,128)(4,1)S(1)} %broadcast_compare_fusion.6, ...), kind=kOutput, calls=%fused_computation.14.clone.1 | convolution fusion | flops 1103888384 | bytes 22077440 | tf_op jit(solution)/shard_map/cond/branch_0_fun/while/body/eval_jaxpr/ths,shd->thd/dot_general | solution.py:33
  358.9 0.7 dynamic_slice.32
  359.6 0.7 iota_add_fusion.5
  360.3 0.8 broadcast_compare_fusion.6
  361.1 4.1 constant_dynamic-slice_fusion.3
  365.1 0.8 dynamic-slice_bitcast_fusion.3
  365.9 7.6 %fusion.87 = (f32[512,4]{0,1:T(4,128)S(1)}, f32[4,2048,512]{2,1,0:T(8,128)}) fusion(f32[4,2048]{1,0:T(4,128)S(1)} %dynamic-slice_bitcast_fusion.3, f32[512,4]{0,1:T(4,128)S(1)} %get-tuple-element.303, pred[512,2048]{0,1:T(8,128)(4,1)S(1)} %broadcast_compare_fusion.6, bf16[512,4,128]{2,0,1:T(8,128)(2,1)S(1)} %copy-done.5, ...), kind=kOutput, calls=%fused_computation.6.clone.1 | convolution fusion | flops 1094711296 | bytes 20496384 | tf_op jit(solution)/shard_map/cond/branch_0_fun/while/body/eval_jaxpr/thd,shd->ths/dot_general | solution.py:21
  373.5 8.8 %fusion.88 = f32[512,4]{0,1:T(4,128)S(1)} fusion(f32[4,2048,512]{2,1,0:T(8,128)} %get-tuple-element.265, f32[512,4]{0,1:T(4,128)S(1)} %select_maximum_fusion.2, f32[4,2048]{1,0:T(4,128)S(1)} %dynamic-slice_bitcast_fusion.3, f32[512,4]{0,1:T(4,128)S(1)} %get-tuple-element.303, pred[512,2048]{0,1:T(8,128)(4,1)S(1)} %broadcast_compare_fusion.6), kind=kLoop, calls=%fused_computation.5.clone.1 | loop fusion | flops 29358080 | bytes 17883136 | tf_op jit(solution)/shard_map/cond/branch_0_fun/while/body/eval_jaxpr/reduce_sum | solution.py:32
  382.3 4.4 copy.46
  386.8 11.0 %fusion.90 = f32[512,4,128]{0,2,1:T(8,128)} fusion(f32[4,2048,512]{2,1,0:T(8,128)} %get-tuple-element.265, f32[512,4]{0,1:T(4,128)S(1)} %select_maximum_fusion.2, f32[4,2048]{1,0:T(4,128)S(1)} %dynamic-slice_bitcast_fusion.3, f32[512,4]{0,1:T(4,128)S(1)} %get-tuple-element.303, pred[512,2048]{0,1:T(8,128)(4,1)S(1)} %broadcast_compare_fusion.6, ...), kind=kOutput, calls=%fused_computation.14.clone.1 | convolution fusion | flops 1103888384 | bytes 22077440 | tf_op jit(solution)/shard_map/cond/branch_0_fun/while/body/eval_jaxpr/ths,shd->thd/dot_general | solution.py:33
  397.7 0.7 dynamic_slice.32
  398.4 0.7 iota_add_fusion.5
  399.1 0.8 broadcast_compare_fusion.6
  399.9 4.1 constant_dynamic-slice_fusion.3
  404.0 0.8 dynamic-slice_bitcast_fusion.3
  404.7 7.6 %fusion.87 = (f32[512,4]{0,1:T(4,128)S(1)}, f32[4,2048,512]{2,1,0:T(8,128)}) fusion(f32[4,2048]{1,0:T(4,128)S(1)} %dynamic-slice_bitcast_fusion.3, f32[512,4]{0,1:T(4,128)S(1)} %get-tuple-element.303, pred[512,2048]{0,1:T(8,128)(4,1)S(1)} %broadcast_compare_fusion.6, bf16[512,4,128]{2,0,1:T(8,128)(2,1)S(1)} %copy-done.5, ...), kind=kOutput, calls=%fused_computation.6.clone.1 | convolution fusion | flops 1094711296 | bytes 20496384 | tf_op jit(solution)/shard_map/cond/branch_0_fun/while/body/eval_jaxpr/thd,shd->ths/dot_general | solution.py:21
  412.4 8.8 %fusion.88 = f32[512,4]{0,1:T(4,128)S(1)} fusion(f32[4,2048,512]{2,1,0:T(8,128)} %get-tuple-element.265, f32[512,4]{0,1:T(4,128)S(1)} %select_maximum_fusion.2, f32[4,2048]{1,0:T(4,128)S(1)} %dynamic-slice_bitcast_fusion.3, f32[512,4]{0,1:T(4,128)S(1)} %get-tuple-element.303, pred[512,2048]{0,1:T(8,128)(4,1)S(1)} %broadcast_compare_fusion.6), kind=kLoop, calls=%fused_computation.5.clone.1 | loop fusion | flops 29358080 | bytes 17883136 | tf_op jit(solution)/shard_map/cond/branch_0_fun/while/body/eval_jaxpr/reduce_sum | solution.py:32
  421.2 4.4 copy.46
  425.6 11.0 %fusion.90 = f32[512,4,128]{0,2,1:T(8,128)} fusion(f32[4,2048,512]{2,1,0:T(8,128)} %get-tuple-element.265, f32[512,4]{0,1:T(4,128)S(1)} %select_maximum_fusion.2, f32[4,2048]{1,0:T(4,128)S(1)} %dynamic-slice_bitcast_fusion.3, f32[512,4]{0,1:T(4,128)S(1)} %get-tuple-element.303, pred[512,2048]{0,1:T(8,128)(4,1)S(1)} %broadcast_compare_fusion.6, ...), kind=kOutput, calls=%fused_computation.14.clone.1 | convolution fusion | flops 1103888384 | bytes 22077440 | tf_op jit(solution)/shard_map/cond/branch_0_fun/while/body/eval_jaxpr/ths,shd->thd/dot_general | solution.py:33
  436.6 1.3 divide_convert_fusion
  438.0 1.3 fusion.64
  439.3 0.4 copy-done.4
  439.7 2.7 fusion.26
  442.5 7.9 %reduce-scatter.2.cloned.1.call-done = bf16[1024,512]{0,1:T(8,128)(2,1)} async-done(((bf16[2048,512]{0,1:T(8,128)(2,1)}), bf16[1024,512]{0,1:T(8,128)(2,1)}) %reduce-scatter.2.cloned.1.call-update) | async-done | bytes 1048592 | tf_op jit(solution)/shard_map/reduce_scatter | solution.py:150
  450.4 1.5 fusion.27
  451.9 2.5 psum.7
  454.4 2.5 fusion.46
  (66 shorter events, 1.5 us)
Async XLA Ops:
  6.5 431.4 %copy-start = (bf16[512,2048]{1,0:T(8,128)(2,1)S(1)}, bf16[512,2048]{1,0:T(8,128)(2,1)}, u32[]{:S(2)}) copy-start(bf16[512,2048]{1,0:T(8,128)(2,1)} %param.25) | copy-start | bytes 6291460
  6.5 15.7 %all-gather.5.cloned.1.call-start = ((), (), s32[]{:S(2)}) async-start(), calls=%async_computation.1 | async-start | bytes 3145728 | tf_op jit(solution)/shard_map/all_gather | solution.py:91
  7.3 134.5 %all-gather.7.cloned.1.call-start = ((), (), s32[]{:S(2)}) async-start(), calls=%async_computation.2 | async-start | bytes 8912896 | tf_op jit(solution)/shard_map/all_gather | solution.py:114
  22.2 2.2 copy-start.2
  28.1 226.9 %all-gather.9.cloned.1.call-start = ((), (), s32[]{:S(2)}) async-start(), calls=%async_computation.3 | async-start | bytes 8912896 | tf_op jit(solution)/shard_map/all_gather | solution.py:115
  32.5 417.9 %reduce-scatter.2.cloned.1.call-start = ((), (), s32[]{:S(2)}) async-start(), calls=%async_computation.4 | async-start | bytes 3145728 | tf_op jit(solution)/shard_map/reduce_scatter | solution.py:150
  33.9 7.3 %copy-start.3 = (bf16[512,2048]{1,0:T(8,128)(2,1)S(1)}, bf16[512,2048]{1,0:T(8,128)(2,1)}, u32[]{:S(2)}) copy-start(bf16[512,2048]{1,0:T(8,128)(2,1)} %all-gather.5.cloned.1.call-done) | copy-start | bytes 6291460
  33.9 7.3 %copy-start.9 = (bf16[2048,512]{1,0:T(8,128)(2,1)S(1)}, bf16[2048,512]{1,0:T(8,128)(2,1)}, u32[]{:S(2)}) copy-start(bf16[2048,512]{1,0:T(8,128)(2,1)} %param.18) | copy-start | bytes 6291460
  37.6 5.2 %collective-permute-start = (bf16[15,512]{1,0:T(8,128)(2,1)S(1)}, bf16[15,512]{1,0:T(8,128)(2,1)S(1)}, u32[]{:S(2)}, u32[]{:S(2)}) collective-permute-start(bf16[15,512]{1,0:T(8,128)(2,1)S(1)} %slice.45), channel_id=1, source_target_pairs={{0,2},{2,4},{4,6},{6,8},{8,10},{10,12},{12,14},{14,16},{16,18},{18... | collective-permute-start | bytes 46088 | tf_op jit(solution)/shard_map/ppermute | solution.py:15
  43.2 0.9 copy-start.10
  44.1 0.9 copy-start.8
  280.1 1.3 copy-start.6
  283.6 4.8 %copy-start.5 = (bf16[512,4,128]{2,0,1:T(8,128)(2,1)S(1)}, bf16[512,4,128]{2,0,1:T(8,128)(2,1)}, u32[]{:S(2)}) copy-start(bf16[512,4,128]{2,0,1:T(8,128)(2,1)} %get-tuple-element.302) | copy-start | bytes 1572868 | tf_op jit(solution)/shard_map/cond/branch_0_fun/while
  322.2 4.8 %copy-start.5 = (bf16[512,4,128]{2,0,1:T(8,128)(2,1)S(1)}, bf16[512,4,128]{2,0,1:T(8,128)(2,1)}, u32[]{:S(2)}) copy-start(bf16[512,4,128]{2,0,1:T(8,128)(2,1)} %get-tuple-element.302) | copy-start | bytes 1572868 | tf_op jit(solution)/shard_map/cond/branch_0_fun/while
  361.0 4.8 %copy-start.5 = (bf16[512,4,128]{2,0,1:T(8,128)(2,1)S(1)}, bf16[512,4,128]{2,0,1:T(8,128)(2,1)}, u32[]{:S(2)}) copy-start(bf16[512,4,128]{2,0,1:T(8,128)(2,1)} %get-tuple-element.302) | copy-start | bytes 1572868 | tf_op jit(solution)/shard_map/cond/branch_0_fun/while
  399.9 4.8 %copy-start.5 = (bf16[512,4,128]{2,0,1:T(8,128)(2,1)S(1)}, bf16[512,4,128]{2,0,1:T(8,128)(2,1)}, u32[]{:S(2)}) copy-start(bf16[512,4,128]{2,0,1:T(8,128)(2,1)} %get-tuple-element.302) | copy-start | bytes 1572868 | tf_op jit(solution)/shard_map/cond/branch_0_fun/while
  438.0 1.3 copy-start.1
  438.0 1.8 copy-start.4
  442.4 11.9 %copy-start.7 = (f32[1024]{0:T(1024)S(1)}, f32[1024]{0:T(1024)}, u32[]{:S(2)}) copy-start(f32[1024]{0:T(1024)} %param.27) | copy-start | bytes 12292
Sparse Core Ops, SparseCore 0:
  8.9 13.2 all-gather.4
  28.3 113.4 all-gather.6
  144.5 110.4 all-gather.8
  442.6 7.7 reduce-scatter.1
where the time goes:
time: 465 us; the launch traced here: 463 us
  waiting for transfers between devices  231 us (50%)
  matrix products  92 us (20%)
  local copies, waits for them, and re-layouts  68.4 us (15%)
  other arithmetic  50.2 us (11%)
  between operations  13.3 us (3%)
    all_gather x1, waiting for transfers between devices, body(): lax.all_gather(values, 'sp', axis=0, tiled=True)  113 us
    all_gather x1, waiting for transfers between devices, body(): lax.all_gather(keys, 'sp', axis=0, tiled=True)  95.9 us
    dot_general x4, matrix products, attend_block(): jnp.einsum('ths,shd->thd', weights.astype(jnp.bfloat16), values, preferre...  43.7 us
    dynamic_slice x12, local copies, waits for them, and re-layouts, attend(): lax.scan(step, state, (keys_blocked, values_blocked, gates_blocked, block...  36.5 us
    reduce_sum x4, other arithmetic, attend_block(): totals = factor * totals + jnp.sum(weights, axis=2)  35.1 us
    dot_general x4, matrix products, attend_block(): jnp.einsum('thd,shd->ths', queries, keys, preferred_element_type=jnp.floa...  30.6 us
    dot_general x4, matrix products, product(): return jnp.dot(scaled, weight, preferred_element_type=jnp.float32)  12.8 us
    all_gather x1, waiting for transfers between devices, body(): part = lax.all_gather(tokens, 'tp', axis=1, tiled=True)  12.8 us
  transfers between devices with their start and end apart: 5, of which 5 were waited for; matrix products, arithmetic and copies ran while one was open for 3% of the time, Pallas kernels for 0%

commit v1 on v0

--- a/solution.py
+++ b/solution.py
@@ -112,7 +112,9 @@
     carry = state
     pieces = (
         lax.all_gather(keys, "sp", axis=0, tiled=True),
-        lax.all_gather(values, "sp", axis=0, tiled=True),
+        jnp.concatenate(
+            lax.all_to_all(jnp.stack([values] * lax.axis_size("sp")), "sp", 0, 0), axis=0
+        ),
     )
     state = lax.cond(
         jnp.int32(0) > last_row,

time: 465 us -> 483 us (1.039)
  waiting for transfers between devices: 231 us -> 272 us
  matrix products: 92 us -> 64.3 us
  other arithmetic: 50.2 us -> 37.9 us
  local copies, waits for them, and re-layouts: 68.4 us -> 77.6 us
  starting transfers between devices: 3.77 us -> 10.7 us
    all_gather x1, waiting for transfers between devices: 95.9 us -> 213 us  [body(): lax.all_gather(keys, 'sp', axis=0, tiled=True)]
    all_gather x1 -> x0, waiting for transfers between devices: 113 us -> none  [body(): lax.all_gather(values, 'sp', axis=0, tiled=True)]
    reduce_scatter x1, waiting for transfers between devices: 7.93 us -> 32.3 us  [body(): lax.psum_scatter((lax.dot_general(attention_out, attended, numbers, prefe...]
    dot_general x4, matrix products: 43.7 us -> 23.3 us  [attend_block(): jnp.einsum('ths,shd->thd', weights.astype(jnp.bfloat16), values, preferre...]
    another operation x1 -> x3, local copies, waits for them, and re-layouts: 0.21 us -> 16.8 us  [the longest x1 12.5 us: attend(): values_blocked = values.reshape(pieces, span, heads, head_size)]
    ppermute x1, waiting for transfers between devices: 0.26 us -> 13.3 us  [passed_along(): return lax.ppermute(block, axis, route)]
    reshape x1 -> x0, local copies, waits for them, and re-layouts: 12.5 us -> none  [attend(): values_blocked = values.reshape(pieces, span, heads, head_size)]
    reduce_sum x4, other arithmetic: 35.1 us -> 22.8 us  [attend_block(): totals = factor * totals + jnp.sum(weights, axis=2)]
  transfers between devices with their start and end apart: 5 -> 5, of which waited for: 5 -> 4; matrix products, arithmetic and copies ran while one was open for 3% -> 3% of each run, Pallas kernels for 0% -> 0%
where the time goes in v1:
time: 483 us; the launch traced here: 481 us
  waiting for transfers between devices  272 us (56%)
  local copies, waits for them, and re-layouts  77.6 us (16%)
  matrix products  64.3 us (13%)
  other arithmetic  37.9 us (8%)
  between operations  13.3 us (3%)
  starting transfers between devices  10.7 us (2%)
    all_gather x1, waiting for transfers between devices, body(): lax.all_gather(keys, 'sp', axis=0, tiled=True)  213 us
    dynamic_slice x12, local copies, waits for them, and re-layouts, attend(): lax.scan(step, state, (keys_blocked, values_blocked, gates_blocked, block...  37.8 us
    reduce_scatter x1, waiting for transfers between devices, body(): lax.psum_scatter((lax.dot_general(attention_out, attended, numbers, prefe...  32.3 us
    dot_general x4, matrix products, attend_block(): jnp.einsum('thd,shd->ths', queries, keys, preferred_element_type=jnp.floa...  24.1 us
    dot_general x4, matrix products, attend_block(): jnp.einsum('ths,shd->thd', weights.astype(jnp.bfloat16), values, preferre...  23.3 us
    reduce_sum x4, other arithmetic, attend_block(): totals = factor * totals + jnp.sum(weights, axis=2)  22.8 us
    ppermute x1, waiting for transfers between devices, passed_along(): return lax.ppermute(block, axis, route)  13.3 us
    all_gather x1, waiting for transfers between devices, body(): part = lax.all_gather(tokens, 'tp', axis=1, tiled=True)  12.8 us
  transfers between devices with their start and end apart: 5, of which 4 were waited for; matrix products, arithmetic and copies ran while one was open for 3% of the time, Pallas kernels for 0%

profile of v1, /device:TPU:0, one launch (start us, length us, event | category | flops | bytes accessed | tf_op | source)
XLA Modules:
  0.0 480.8 jit_solution(10107909684643783107)
XLA Ops:
  6.5 0.7 all-gather.4.cloned.1.call-update
  7.3 2.1 all-gather
  9.4 12.8 %all-gather.4.cloned.1.call-done = bf16[512,2048]{1,0:T(8,128)(2,1)} async-done(((bf16[512,1024]{1,0:T(8,128)(2,1)}), bf16[512,2048]{1,0:T(8,128)(2,1)}) %all-gather.4.cloned.1.call-update) | async-done | bytes 2097168 | tf_op jit(solution)/shard_map/all_gather | solution.py:91
  22.2 2.2 fusion.25
  24.5 3.7 fusion.34
  28.1 3.5 fusion.37
  31.6 4.0 stack.2
  35.7 6.8 %all-to-all-start = ((bf16[16,512,512]{2,1,0:T(8,128)(2,1)}), bf16[16,512,512]{2,1,0:T(8,128)(2,1)}, u32[]{:S(2)}, u32[]{:S(2)}) async-start(bf16[16,512,512]{2,1,0:T(8,128)(2,1)} %stack.2), calls=%async_computation | async-start | bytes 16777216 | tf_op jit(solution)/shard_map/all_to_all | solution.py:116
  42.6 1.3 dynamic-slice_bitcast_fusion.1
  43.9 3.6 fusion.43
  47.6 3.8 collective-permute-start
  51.4 1.3 fusion.40
  52.7 13.3 %collective-permute-done = bf16[15,512]{1,0:T(8,128)(2,1)S(1)} collective-permute-done((bf16[15,512]{1,0:T(8,128)(2,1)S(1)}, bf16[15,512]{1,0:T(8,128)(2,1)S(1)}, u32[]{:S(2)}, u32[]{:S(2)}) %collective-permute-start) | collective-permute-done | bytes 15392 | tf_op jit(solution)/shard_map/ppermute | solution.py:15
  66.6 0.7 copy-done.12
  67.3 0.8 fusion.54
  68.2 1.0 fusion.52
  69.2 213.0 %all-gather.6.cloned.1.call-done = bf16[8192,512]{1,0:T(8,128)(2,1)} async-done(((bf16[512,512]{1,0:T(8,128)(2,1)}), bf16[8192,512]{1,0:T(8,128)(2,1)}) %all-gather.6.cloned.1.call-update) | async-done | bytes 8388624 | tf_op jit(solution)/shard_map/all_gather | solution.py:114
  282.1 147.5 %conditional.1 = (f32[512,4]{0,1:T(4,128)S(1)}, f32[512,4,128]{0,2,1:T(8,128)}) conditional(s32[]{:T(128)} %convert_element_type.58, (bf16[8192,512]{1,0:T(8,128)(2,1)}, bf16[16,512,512]{2,1,0:T(8,128)(2,1)}, f32[4,8192]{1,0:T(4,128)}, bf16[512,512]{1,0:T(8,128)(2,1)S(1)}, s32[]{:T(128)}, /*index=5*/f32[512,4]{0,1:T(4,128)}) %tuple.17, () %tuple.18), branch_computations={%region_1.6_spmd, %region_6.7_spmd} | conditional | flops 2229023232 | bytes 126726560 | solution.py:119
  282.3 1.0 copy.25
  283.3 12.5 %reshape_reshape.2 = bf16[4,2048,4,128]{3,2,1,0:T(4,128)(2,1)} reshape(bf16[16,512,512]{2,1,0:T(8,128)(2,1)} %get-tuple-element.79) | data formatting | bytes 16777216 | tf_op jit(solution)/shard_map/cond/branch_0_fun/reshape;reshape | solution.py:49
  295.9 12.6 %reshape.108 = bf16[4,2048,4,128]{3,2,1,0:T(4,128)(2,1)} reshape(bf16[8192,512]{1,0:T(8,128)(2,1)} %get-tuple-element.75) | data formatting | bytes 16777216 | tf_op jit(solution)/shard_map/cond/branch_0_fun/reshape | solution.py:48
  308.5 121.2 %while.14 = (s32[]{:T(128)}, f32[512,4]{0,1:T(4,128)S(1)}, f32[512,4]{0,1:T(4,128)S(1)}, f32[512,4,128]{0,2,1:T(8,128)}, s32[]{:T(128)}, /*index=5*/s32[4]{0:T(1...) while((s32[]{:T(128)}, f32[512,4]{0,1:T(4,128)S(1)}, ...), condition=%wide.region_5.5_spmd.clone, body=%wide.region_2.4_spmd.clone.sunk | while | flops 2229023232 | bytes 91042040 | solution.py:61
  309.1 0.7 iota_add_fusion.5
  309.8 0.8 dynamic-slice_bitcast_fusion.3
  310.6 0.7 broadcast_compare_fusion.6
  311.4 4.4 constant_dynamic-slice_fusion.3
  315.8 4.3 copy.46
  320.1 6.0 %fusion.87 = (f32[512,4]{0,1:T(4,128)S(1)}, f32[4,2048,512]{2,1,0:T(8,128)S(1)}) fusion(f32[4,2048]{1,0:T(4,128)S(1)} %dynamic-slice_bitcast_fusion.3, f32[512,4]{0,1:T(4,128)S(1)} %get-tuple-element.303, pred[512,2048]{0,1:T(8,128)(4,1)S(1)} %broadcast_compare_fusion.6, bf16[512,4,128]{2,0,1:T(8,128)(2,1)} %get-tuple-element.302, ...), kind=kOutput, calls=%fused_computation.6.clone.1 | convolution fusion | flops 1094711296 | bytes 20496384 | tf_op jit(solution)/shard_map/cond/branch_0_fun/while/body/eval_jaxpr/thd,shd->ths/dot_general | solution.py:21
  326.2 5.7 %fusion.88 = f32[512,4]{0,1:T(4,128)S(1)} fusion(f32[4,2048,512]{2,1,0:T(8,128)S(1)} %get-tuple-element.265, f32[512,4]{0,1:T(4,128)S(1)} %select_maximum_fusion.2, f32[4,2048]{1,0:T(4,128)S(1)} %dynamic-slice_bitcast_fusion.3, f32[512,4]{0,1:T(4,128)S(1)} %get-tuple-element.303, pred[512,2048]{0,1:T(8,128)(4,1)S(1)} %broadcast_compare_fusion.6), kind=kLoop, calls=%fused_computation.5.clone.1 | loop fusion | flops 29358080 | bytes 17883136 | tf_op jit(solution)/shard_map/cond/branch_0_fun/while/body/eval_jaxpr/reduce_sum | solution.py:32
  331.9 5.8 %fusion.90 = f32[512,4,128]{0,2,1:T(8,128)S(1)} fusion(f32[4,2048,512]{2,1,0:T(8,128)S(1)} %get-tuple-element.265, f32[512,4]{0,1:T(4,128)S(1)} %select_maximum_fusion.2, f32[4,2048]{1,0:T(4,128)S(1)} %dynamic-slice_bitcast_fusion.3, f32[512,4]{0,1:T(4,128)S(1)} %get-tuple-element.303, pred[512,2048]{0,1:T(8,128)(4,1)S(1)} %broadcast_compare_fusion.6, ...), kind=kOutput, calls=%fused_computation.14.clone.1 | convolution fusion | flops 1103888384 | bytes 22077440 | tf_op jit(solution)/shard_map/cond/branch_0_fun/while/body/eval_jaxpr/ths,shd->thd/dot_general | solution.py:33
  337.8 0.9 copy-done.7
  339.4 0.7 iota_add_fusion.5
  340.1 0.8 dynamic-slice_bitcast_fusion.3
  340.9 0.7 broadcast_compare_fusion.6
  341.6 4.4 constant_dynamic-slice_fusion.3
  346.1 4.3 copy.46
  350.4 6.0 %fusion.87 = (f32[512,4]{0,1:T(4,128)S(1)}, f32[4,2048,512]{2,1,0:T(8,128)S(1)}) fusion(f32[4,2048]{1,0:T(4,128)S(1)} %dynamic-slice_bitcast_fusion.3, f32[512,4]{0,1:T(4,128)S(1)} %get-tuple-element.303, pred[512,2048]{0,1:T(8,128)(4,1)S(1)} %broadcast_compare_fusion.6, bf16[512,4,128]{2,0,1:T(8,128)(2,1)} %get-tuple-element.302, ...), kind=kOutput, calls=%fused_computation.6.clone.1 | convolution fusion | flops 1094711296 | bytes 20496384 | tf_op jit(solution)/shard_map/cond/branch_0_fun/while/body/eval_jaxpr/thd,shd->ths/dot_general | solution.py:21
  356.5 5.7 %fusion.88 = f32[512,4]{0,1:T(4,128)S(1)} fusion(f32[4,2048,512]{2,1,0:T(8,128)S(1)} %get-tuple-element.265, f32[512,4]{0,1:T(4,128)S(1)} %select_maximum_fusion.2, f32[4,2048]{1,0:T(4,128)S(1)} %dynamic-slice_bitcast_fusion.3, f32[512,4]{0,1:T(4,128)S(1)} %get-tuple-element.303, pred[512,2048]{0,1:T(8,128)(4,1)S(1)} %broadcast_compare_fusion.6), kind=kLoop, calls=%fused_computation.5.clone.1 | loop fusion | flops 29358080 | bytes 17883136 | tf_op jit(solution)/shard_map/cond/branch_0_fun/while/body/eval_jaxpr/reduce_sum | solution.py:32
  362.2 5.8 %fusion.90 = f32[512,4,128]{0,2,1:T(8,128)S(1)} fusion(f32[4,2048,512]{2,1,0:T(8,128)S(1)} %get-tuple-element.265, f32[512,4]{0,1:T(4,128)S(1)} %select_maximum_fusion.2, f32[4,2048]{1,0:T(4,128)S(1)} %dynamic-slice_bitcast_fusion.3, f32[512,4]{0,1:T(4,128)S(1)} %get-tuple-element.303, pred[512,2048]{0,1:T(8,128)(4,1)S(1)} %broadcast_compare_fusion.6, ...), kind=kOutput, calls=%fused_computation.14.clone.1 | convolution fusion | flops 1103888384 | bytes 22077440 | tf_op jit(solution)/shard_map/cond/branch_0_fun/while/body/eval_jaxpr/ths,shd->thd/dot_general | solution.py:33
  368.1 0.9 copy-done.7
  370.4 0.8 dynamic-slice_bitcast_fusion.3
  371.2 0.7 broadcast_compare_fusion.6
  371.9 4.4 constant_dynamic-slice_fusion.3
  376.4 4.3 copy.46
  380.7 6.0 %fusion.87 = (f32[512,4]{0,1:T(4,128)S(1)}, f32[4,2048,512]{2,1,0:T(8,128)S(1)}) fusion(f32[4,2048]{1,0:T(4,128)S(1)} %dynamic-slice_bitcast_fusion.3, f32[512,4]{0,1:T(4,128)S(1)} %get-tuple-element.303, pred[512,2048]{0,1:T(8,128)(4,1)S(1)} %broadcast_compare_fusion.6, bf16[512,4,128]{2,0,1:T(8,128)(2,1)} %get-tuple-element.302, ...), kind=kOutput, calls=%fused_computation.6.clone.1 | convolution fusion | flops 1094711296 | bytes 20496384 | tf_op jit(solution)/shard_map/cond/branch_0_fun/while/body/eval_jaxpr/thd,shd->ths/dot_general | solution.py:21
  386.8 5.7 %fusion.88 = f32[512,4]{0,1:T(4,128)S(1)} fusion(f32[4,2048,512]{2,1,0:T(8,128)S(1)} %get-tuple-element.265, f32[512,4]{0,1:T(4,128)S(1)} %select_maximum_fusion.2, f32[4,2048]{1,0:T(4,128)S(1)} %dynamic-slice_bitcast_fusion.3, f32[512,4]{0,1:T(4,128)S(1)} %get-tuple-element.303, pred[512,2048]{0,1:T(8,128)(4,1)S(1)} %broadcast_compare_fusion.6), kind=kLoop, calls=%fused_computation.5.clone.1 | loop fusion | flops 29358080 | bytes 17883136 | tf_op jit(solution)/shard_map/cond/branch_0_fun/while/body/eval_jaxpr/reduce_sum | solution.py:32
  392.5 5.8 %fusion.90 = f32[512,4,128]{0,2,1:T(8,128)S(1)} fusion(f32[4,2048,512]{2,1,0:T(8,128)S(1)} %get-tuple-element.265, f32[512,4]{0,1:T(4,128)S(1)} %select_maximum_fusion.2, f32[4,2048]{1,0:T(4,128)S(1)} %dynamic-slice_bitcast_fusion.3, f32[512,4]{0,1:T(4,128)S(1)} %get-tuple-element.303, pred[512,2048]{0,1:T(8,128)(4,1)S(1)} %broadcast_compare_fusion.6, ...), kind=kOutput, calls=%fused_computation.14.clone.1 | convolution fusion | flops 1103888384 | bytes 22077440 | tf_op jit(solution)/shard_map/cond/branch_0_fun/while/body/eval_jaxpr/ths,shd->thd/dot_general | solution.py:33
  398.4 0.9 copy-done.7
  400.0 0.7 iota_add_fusion.5
  400.7 0.8 dynamic-slice_bitcast_fusion.3
  401.5 0.7 broadcast_compare_fusion.6
  402.2 4.4 constant_dynamic-slice_fusion.3
  406.7 4.3 copy.46
  411.0 6.0 %fusion.87 = (f32[512,4]{0,1:T(4,128)S(1)}, f32[4,2048,512]{2,1,0:T(8,128)S(1)}) fusion(f32[4,2048]{1,0:T(4,128)S(1)} %dynamic-slice_bitcast_fusion.3, f32[512,4]{0,1:T(4,128)S(1)} %get-tuple-element.303, pred[512,2048]{0,1:T(8,128)(4,1)S(1)} %broadcast_compare_fusion.6, bf16[512,4,128]{2,0,1:T(8,128)(2,1)} %get-tuple-element.302, ...), kind=kOutput, calls=%fused_computation.6.clone.1 | convolution fusion | flops 1094711296 | bytes 20496384 | tf_op jit(solution)/shard_map/cond/branch_0_fun/while/body/eval_jaxpr/thd,shd->ths/dot_general | solution.py:21
  417.1 5.7 %fusion.88 = f32[512,4]{0,1:T(4,128)S(1)} fusion(f32[4,2048,512]{2,1,0:T(8,128)S(1)} %get-tuple-element.265, f32[512,4]{0,1:T(4,128)S(1)} %select_maximum_fusion.2, f32[4,2048]{1,0:T(4,128)S(1)} %dynamic-slice_bitcast_fusion.3, f32[512,4]{0,1:T(4,128)S(1)} %get-tuple-element.303, pred[512,2048]{0,1:T(8,128)(4,1)S(1)} %broadcast_compare_fusion.6), kind=kLoop, calls=%fused_computation.5.clone.1 | loop fusion | flops 29358080 | bytes 17883136 | tf_op jit(solution)/shard_map/cond/branch_0_fun/while/body/eval_jaxpr/reduce_sum | solution.py:32
  422.8 5.8 %fusion.90 = f32[512,4,128]{0,2,1:T(8,128)S(1)} fusion(f32[4,2048,512]{2,1,0:T(8,128)S(1)} %get-tuple-element.265, f32[512,4]{0,1:T(4,128)S(1)} %select_maximum_fusion.2, f32[4,2048]{1,0:T(4,128)S(1)} %dynamic-slice_bitcast_fusion.3, f32[512,4]{0,1:T(4,128)S(1)} %get-tuple-element.303, pred[512,2048]{0,1:T(8,128)(4,1)S(1)} %broadcast_compare_fusion.6, ...), kind=kOutput, calls=%fused_computation.14.clone.1 | convolution fusion | flops 1103888384 | bytes 22077440 | tf_op jit(solution)/shard_map/cond/branch_0_fun/while/body/eval_jaxpr/ths,shd->thd/dot_general | solution.py:33
  428.7 0.9 copy-done.7
  429.7 1.3 divide_convert_fusion
  431.0 1.3 fusion.64
  432.8 2.7 fusion.26
  435.5 32.3 %reduce-scatter.2.cloned.1.call-done = bf16[1024,512]{0,1:T(8,128)(2,1)} async-done(((bf16[2048,512]{0,1:T(8,128)(2,1)}), bf16[1024,512]{0,1:T(8,128)(2,1)}) %reduce-scatter.2.cloned.1.call-update) | async-done | bytes 1048592 | tf_op jit(solution)/shard_map/reduce_scatter | solution.py:152
  467.8 1.5 fusion.27
  469.3 2.5 psum.7
  471.8 2.5 fusion.46
  (82 shorter events, 5.0 us)
Async XLA Ops:
  6.5 424.5 %copy-start = (bf16[512,2048]{1,0:T(8,128)(2,1)S(1)}, bf16[512,2048]{1,0:T(8,128)(2,1)}, u32[]{:S(2)}) copy-start(bf16[512,2048]{1,0:T(8,128)(2,1)} %param.25) | copy-start | bytes 6291460
  6.5 15.7 %all-gather.4.cloned.1.call-start = ((), (), s32[]{:S(2)}) async-start(), calls=%async_computation.2 | async-start | bytes 3145728 | tf_op jit(solution)/shard_map/all_gather | solution.py:91
  7.3 274.9 %all-gather.6.cloned.1.call-start = ((), (), s32[]{:S(2)}) async-start(), calls=%async_computation.3 | async-start | bytes 8912896 | tf_op jit(solution)/shard_map/all_gather | solution.py:114
  22.2 2.2 copy-start.3
  35.7 246.5 %all-to-all-start = ((bf16[16,512,512]{2,1,0:T(8,128)(2,1)}), bf16[16,512,512]{2,1,0:T(8,128)(2,1)}, u32[]{:S(2)}, u32[]{:S(2)}) async-start(bf16[16,512,512]{2,1,0:T(8,128)(2,1)} %stack.2), calls=%async_computation | async-start | bytes 16777216 | tf_op jit(solution)/shard_map/all_to_all | solution.py:116
  42.5 425.3 %reduce-scatter.2.cloned.1.call-start = ((), (), s32[]{:S(2)}) async-start(), calls=%async_computation.4 | async-start | bytes 3145728 | tf_op jit(solution)/shard_map/reduce_scatter | solution.py:152
  43.9 7.5 %copy-start.4 = (bf16[512,2048]{1,0:T(8,128)(2,1)S(1)}, bf16[512,2048]{1,0:T(8,128)(2,1)}, u32[]{:S(2)}) copy-start(bf16[512,2048]{1,0:T(8,128)(2,1)} %all-gather.4.cloned.1.call-done) | copy-start | bytes 6291460
  43.9 7.5 %copy-start.11 = (bf16[2048,512]{1,0:T(8,128)(2,1)S(1)}, bf16[2048,512]{1,0:T(8,128)(2,1)}, u32[]{:S(2)}) copy-start(bf16[2048,512]{1,0:T(8,128)(2,1)} %param.18) | copy-start | bytes 6291460
  47.6 18.4 %collective-permute-start = (bf16[15,512]{1,0:T(8,128)(2,1)S(1)}, bf16[15,512]{1,0:T(8,128)(2,1)S(1)}, u32[]{:S(2)}, u32[]{:S(2)}) collective-permute-start(bf16[15,512]{1,0:T(8,128)(2,1)S(1)} %slice.45), channel_id=1, source_target_pairs={{0,2},{2,4},{4,6},{6,8},{8,10},{10,12},{12,14},{14,16},{16,18},{18... | collective-permute-start | bytes 46088 | tf_op jit(solution)/shard_map/ppermute | solution.py:15
  66.4 0.9 copy-start.12
  67.3 0.9 copy-start.10
  295.9 12.6 %copy-start.8 = (f32[512,4]{0,1:T(4,128)S(1)}, f32[512,4]{0,1:T(4,128)}, u32[]{:S(2)}) copy-start(f32[512,4]{0,1:T(4,128)} %get-tuple-element.277) | copy-start | bytes 24580 | tf_op jit(solution)/shard_map/cond
  326.2 5.8 %copy-start.1 = (bf16[1,2048,4,128]{1,3,2,0:T(8,128)(2,1)S(1)}, bf16[1,2048,4,128]{1,3,2,0:T(8,128)(2,1)}, u32[]{:S(2)}) copy-start(bf16[1,2048,4,128]{1,3,2,0:T(8,128)(2,1)} %copy.46) | copy-start | bytes 6291460 | tf_op jit(solution)/shard_map/cond/branch_0_fun/while
  326.2 5.8 %copy-start.6 = (f32[512,4,128]{0,2,1:T(8,128)S(1)}, f32[512,4,128]{0,2,1:T(8,128)}, u32[]{:S(2)}) copy-start(f32[512,4,128]{0,2,1:T(8,128)} %get-tuple-element.285) | copy-start | bytes 3145732 | tf_op jit(solution)/shard_map/cond/branch_0_fun/while
  337.8 1.0 copy-start.7
  356.5 5.8 %copy-start.1 = (bf16[1,2048,4,128]{1,3,2,0:T(8,128)(2,1)S(1)}, bf16[1,2048,4,128]{1,3,2,0:T(8,128)(2,1)}, u32[]{:S(2)}) copy-start(bf16[1,2048,4,128]{1,3,2,0:T(8,128)(2,1)} %copy.46) | copy-start | bytes 6291460 | tf_op jit(solution)/shard_map/cond/branch_0_fun/while
  356.5 5.8 %copy-start.6 = (f32[512,4,128]{0,2,1:T(8,128)S(1)}, f32[512,4,128]{0,2,1:T(8,128)}, u32[]{:S(2)}) copy-start(f32[512,4,128]{0,2,1:T(8,128)} %get-tuple-element.285) | copy-start | bytes 3145732 | tf_op jit(solution)/shard_map/cond/branch_0_fun/while
  368.1 1.0 copy-start.7
  386.8 5.8 %copy-start.1 = (bf16[1,2048,4,128]{1,3,2,0:T(8,128)(2,1)S(1)}, bf16[1,2048,4,128]{1,3,2,0:T(8,128)(2,1)}, u32[]{:S(2)}) copy-start(bf16[1,2048,4,128]{1,3,2,0:T(8,128)(2,1)} %copy.46) | copy-start | bytes 6291460 | tf_op jit(solution)/shard_map/cond/branch_0_fun/while
  386.8 5.8 %copy-start.6 = (f32[512,4,128]{0,2,1:T(8,128)S(1)}, f32[512,4,128]{0,2,1:T(8,128)}, u32[]{:S(2)}) copy-start(f32[512,4,128]{0,2,1:T(8,128)} %get-tuple-element.285) | copy-start | bytes 3145732 | tf_op jit(solution)/shard_map/cond/branch_0_fun/while
  398.4 1.0 copy-start.7
  417.1 5.8 %copy-start.1 = (bf16[1,2048,4,128]{1,3,2,0:T(8,128)(2,1)S(1)}, bf16[1,2048,4,128]{1,3,2,0:T(8,128)(2,1)}, u32[]{:S(2)}) copy-start(bf16[1,2048,4,128]{1,3,2,0:T(8,128)(2,1)} %copy.46) | copy-start | bytes 6291460 | tf_op jit(solution)/shard_map/cond/branch_0_fun/while
  417.1 5.8 %copy-start.6 = (f32[512,4,128]{0,2,1:T(8,128)S(1)}, f32[512,4,128]{0,2,1:T(8,128)}, u32[]{:S(2)}) copy-start(f32[512,4,128]{0,2,1:T(8,128)} %get-tuple-element.285) | copy-start | bytes 3145732 | tf_op jit(solution)/shard_map/cond/branch_0_fun/while
  428.7 1.0 copy-start.7
  431.0 1.3 copy-start.2
  431.0 1.8 copy-start.5
  435.5 36.3 %copy-start.9 = (f32[1024]{0:T(1024)S(1)}, f32[1024]{0:T(1024)}, u32[]{:S(2)}) copy-start(f32[1024]{0:T(1024)} %param.27) | copy-start | bytes 12292
Sparse Core Ops, SparseCore 0:
  8.9 13.2 all-gather.3
  28.3 253.8 all-gather.5
  435.6 32.1 reduce-scatter.1
